TPU v7x, 128 devices: a whole 4x4x4 slice. The times are simulated.
128 devices in a mesh: sp: 64 (over z, y, x), tp: 2 (over core).
Axes of the slice: x: 4, y: 4, z: 4, core: 2. Of those that a mesh axis runs over, the one named last changes fastest.
Arguments:
- tokens: bfloat16 [32768, 4096], P(('sp', 'tp')), may hold values from -6 to 6
- norm_gain: float32 [4096], replicated, may hold values from 0.5 to 1.5
- query_weight: bfloat16 [4096, 1024], P(None, 'tp'), may hold values from -0.09375 to 0.09375
- key_weight: bfloat16 [4096, 1024], P(None, 'tp'), may hold values from -0.09375 to 0.09375
- value_weight: bfloat16 [4096, 2048], P(None, 'tp'), may hold values from -0.09375 to 0.09375
- gate_weight: bfloat16 [4096, 2048], P(None, 'tp'), may hold values from -0.09375 to 0.09375
- decay_bias: float32 [1024], P('tp'), may hold values from -0.5 to 0.5
- head_gain: float32 [2048], P('tp'), may hold values from 0.5 to 1.5
- out_weight: bfloat16 [2048, 4096], P('tp'), may hold values from -0.125 to 0.125
Outputs:
- layer_out: bfloat16 [32768, 4096], P(('sp', 'tp'))
All inputs are finite; a program needn't handle non-finite values.
Results may differ from a plain program's by a relative error of at most 0.015.
Values may be sent and summed in bfloat16 or wider, within the bound.
No kernel may reach another device: no remote copies, remote signals or barrier semaphores. Data moves between devices by JAX's collectives and lax.ppermute only.
A program may use at most 192 MiB of HBM per device.

v0:
```python
import math

import jax
import jax.numpy as jnp
from jax import lax
from jax.sharding import Mesh
from jax.sharding import PartitionSpec as P

HEAD_K = 128
HEAD_V = 256
BLOCK = 64
SP = ("sp_0", "sp_1", "sp_2")
SP_TP = ("sp_0", "sp_1", "sp_2", "tp")


epsilon = 1e-06
decay_power = 16.0
precise = lax.Precision.HIGHEST


def gathered_then(shard, axis, dim, work):
    return work(lax.all_gather(shard, axis, axis=dim, tiled=True), jnp.int32(0))


def filled_with(x, identity):
    return jax.tree.map(
        lambda a, e: jnp.broadcast_to(jnp.asarray(e, a.dtype), a.shape), x, identity
    )


def carried_in_2(x, axes, combine, identity, reverse):
    before = start = filled_with(x, identity)
    total = x
    for axis in reversed(axes):
        devices, position = lax.axis_size(axis), lax.axis_index(axis)
        pieces = jax.tree.map(lambda part: lax.all_gather(part, axis), total)
        inside, total = start, start
        for k in reversed(range(devices)) if reverse else range(devices):
            passed = k > position if reverse else k < position
            total = combine(total, jax.tree.map(lambda part: part[k], pieces))
            inside = jax.tree.map(lambda new, old: jnp.where(passed, new, old), total, inside)
        before = combine(inside, before)
    return before


def own_rows(portion, extent, axis):
    count = extent * lax.axis_size(axis)
    sent = portion(jnp.int32(0), count).astype(jnp.bfloat16)
    return lax.psum_scatter(sent, axis, scatter_dimension=0, tiled=True).astype(jnp.float32)


def to_blocks(values, head_width):
    block_count = values.shape[0] // BLOCK
    head_count = values.shape[1] // head_width
    return (
        values.astype(jnp.float32)
        .reshape(block_count, BLOCK, head_count, head_width)
        .transpose(2, 0, 1, 3)
    )


def combine(earlier_part, later_part):
    return (
        earlier_part[0] * later_part[0],
        later_part[0][..., None] * earlier_part[1] + later_part[1],
    )


def local_pass(queries, key_rows, value_rows, within, totals, start_state):
    block_end = totals[:, :, None, :]
    query_in = queries * jnp.exp(within)
    key_in = key_rows * jnp.exp(-within)
    key_out = key_rows * jnp.exp(block_end - within)
    causal = jnp.tril(jnp.ones((BLOCK, BLOCK), dtype=bool))
    scores = jnp.where(
        causal, jnp.einsum("hnid,hnjd->hnij", query_in, key_in, precision=precise), 0.0
    )
    local_out = jnp.einsum("hnij,hnjv->hniv", scores, value_rows, precision=precise)
    block_decay = jnp.exp(totals)

    def advance(carry_state, inputs_now):
        query_now, key_now, value_now, decay_now = inputs_now
        carried = jnp.einsum("hid,hdv->hiv", query_now, carry_state, precision=precise)
        carry_state = decay_now[..., None] * carry_state + jnp.einsum(
            "hjd,hjv->hdv", key_now, value_now, precision=precise
        )
        return (carry_state, carried)

    sequence_inputs = (
        jnp.moveaxis(query_in, 1, 0),
        jnp.moveaxis(key_out, 1, 0),
        jnp.moveaxis(value_rows, 1, 0),
        jnp.moveaxis(block_decay, 1, 0),
    )
    final_state, carried_out = lax.scan(advance, start_state, sequence_inputs)
    return (local_out + jnp.moveaxis(carried_out, 0, 1), final_state)


def mix_heads(queries, key_rows, value_rows, log_decay, carry):
    within = jnp.cumsum(log_decay, axis=2)
    totals = within[:, :, -1, :]
    before = jnp.cumsum(totals, axis=1) - totals
    span_end = before[:, -1, :] + totals[:, -1, :]
    through = within + before[:, :, None, :]
    key_out = key_rows * jnp.exp(span_end[:, None, None, :] - through)
    state_here = jnp.einsum("hncd,hncv->hdv", key_out, value_rows, precision=precise)
    carried_in = carry(jnp.exp(span_end), state_here)
    mixed_out, final_state = local_pass(queries, key_rows, value_rows, within, totals, carried_in)
    return mixed_out


def on_device(
    tokens,
    norm_gain,
    query_weight,
    key_weight,
    value_weight,
    gate_weight,
    decay_bias,
    head_gain,
    out_weight,
):
    inputs = tokens.astype(jnp.float32)
    row_scale = lax.rsqrt(jnp.mean(inputs * inputs, axis=-1, keepdims=True) + epsilon)
    normed = (inputs * row_scale * norm_gain.astype(jnp.float32)).astype(jnp.bfloat16)
    weights = (query_weight, key_weight, value_weight, gate_weight)

    def project(row_piece, row_start):
        return jnp.concatenate(
            [
                jnp.dot(row_piece, matrix, preferred_element_type=jnp.float32).astype(jnp.bfloat16)
                for matrix in weights
            ],
            axis=1,
        )

    projected = gathered_then(normed, "tp", 0, project)
    key_width = query_weight.shape[1]
    value_width = value_weight.shape[1]
    query_flat = projected[:, :key_width]
    key_flat = projected[:, key_width : 2 * key_width]
    value_flat = projected[:, 2 * key_width : 2 * key_width + value_width]
    gate_input = projected[:, 2 * key_width + value_width : 2 * key_width + 2 * value_width]
    span_rows = projected.shape[0]
    sequence = lax.axis_size(SP) * span_rows
    logits = decay_bias.astype(jnp.float32) + math.log(sequence / 8.0)
    log_decay = jnp.broadcast_to(jax.nn.log_sigmoid(logits) / decay_power, (span_rows, key_width))
    queries = to_blocks(query_flat, HEAD_K) * HEAD_K ** (-0.5)
    key_blocks = to_blocks(key_flat, HEAD_K)
    value_blocks = to_blocks(value_flat, HEAD_V)
    decay_blocks = to_blocks(log_decay, HEAD_K)
    head_count = queries.shape[0]

    def carry_all(span_decay, span_state):
        return carried_in_2(
            (span_decay, span_state),
            SP,
            combine,
            (jnp.ones_like(span_decay), jnp.zeros_like(span_state)),
            False,
        )[1]

    mixed_heads = mix_heads(queries, key_blocks, value_blocks, decay_blocks, carry_all)
    mixed_heads = mixed_heads.transpose(1, 2, 0, 3).reshape(span_rows, head_count, HEAD_V)
    head_scale = lax.rsqrt(jnp.mean(mixed_heads * mixed_heads, axis=-1, keepdims=True) + epsilon)
    normed_heads = (
        mixed_heads * head_scale * head_gain.astype(jnp.float32).reshape(head_count, HEAD_V)
    ).reshape(span_rows, head_count * HEAD_V)
    gated_rows = (normed_heads * jax.nn.silu(gate_input.astype(jnp.float32))).astype(jnp.bfloat16)
    rows_here = tokens.shape[0]

    def project_out(first_row, row_count):
        return jnp.dot(
            lax.dynamic_slice_in_dim(gated_rows, first_row, row_count, 0),
            out_weight,
            preferred_element_type=jnp.float32,
        )

    summed = own_rows(project_out, rows_here, "tp")
    return summed.astype(jnp.bfloat16)


def solution(mesh):
    finer = Mesh(mesh.devices.reshape(4, 4, 4, mesh.shape["tp"]), ("sp_0", "sp_1", "sp_2", "tp"))
    in_specs = (
        P(SP_TP, None),
        P(),
        P(None, "tp"),
        P(None, "tp"),
        P(None, "tp"),
        P(None, "tp"),
        P("tp"),
        P("tp"),
        P("tp", None),
    )
    out_specs = P(SP_TP, None)
    return jax.shard_map(
        on_device, mesh=finer, in_specs=in_specs, out_specs=out_specs, check_vma=False
    )
```

profile of v0, /device:TPU:1, one launch (start us, length us, event | category | flops | bytes accessed | tf_op | source)
XLA Modules:
  0.0 250.6 jit_solution(1708266083529635104)
XLA Ops:
  6.5 2.2 fusion.4
  8.8 2.7 %fusion.6 = bf16[256,4096]{1,0:T(8,128)(2,1)} fusion(bf16[256,4096]{1,0:T(8,128)(2,1)S(1)} %copy-done.3, f32[4096]{0:T(1024)} %param.12, f32[256]{0:T(256)S(1)} %add_rsqrt_fusion.1), kind=kLoop, calls=%fused_computation.14 | loop fusion | flops 4194304 | bytes 4211712 | tf_op jit(solution)/shard_map/convert_element_type | solution.py:125
  11.5 0.0 all-gather.7.cloned.1.call-update
  11.5 0.0 all-gather.13.cloned.1.call-start
  11.5 0.6 copy-done.8
  12.2 19.5 %all-gather.7.cloned.1.call-done = bf16[512,4096]{1,0:T(8,128)(2,1)} async-done(((bf16[256,4096]{1,0:T(8,128)(2,1)}), bf16[512,4096]{1,0:T(8,128)(2,1)}) %all-gather.7.cloned.1.call-update) | async-done | bytes 4194320 | tf_op jit(solution)/shard_map/all_gather | solution.py:22
  31.6 5.8 %fusion.12 = f32[512,512]{1,0:T(8,128)S(1)} fusion(bf16[512,4096]{1,0:T(8,128)(2,1)} %all-gather.7.cloned.1.call-done, bf16[4096,512]{1,0:T(8,128)(2,1)} %param.14), kind=kOutput, calls=%fused_computation.29 | convolution fusion | flops 2148007936 | bytes 9437184 | tf_op jit(solution)/shard_map/dot_general | solution.py:131
  37.4 0.4 reshape.176
  37.8 5.8 %fusion.14 = f32[512,512]{1,0:T(8,128)S(1)} fusion(bf16[512,4096]{1,0:T(8,128)(2,1)} %all-gather.7.cloned.1.call-done, bf16[4096,512]{1,0:T(8,128)(2,1)} %param.13), kind=kOutput, calls=%fused_computation.32 | convolution fusion | flops 2148270080 | bytes 9437184 | tf_op jit(solution)/shard_map/dot_general | solution.py:131
  43.6 0.4 mul.334
  44.0 2.6 %bitcast_multiply_fusion.4 = (f32[4,8,64,128]{3,1,2,0:T(8,128)}, f32[4,8,64,128]{3,1,2,0:T(8,128)}, f32[4,8,64,128]{3,1,2,0:T(8,128)S(1)}) fusion(f32[8,64,4,128]{3,2,1,0:T(4,128)S(1)} %mul.334, f32[8,64,4,128]{3,2,1,0:T(4,128)S(1)} %reshape.176, f32[4,128]{1,0:T(4,128)S(1)} %fusion.47), kind=kOutput, calls=%fused_computation.44 | output fusion | flops 17301504 | bytes 5244928 | tf_op jit(solution)/shard_map/jit(cumsum)/reduce_window_sum | solution.py:100
  46.7 10.1 %convolution_convert_fusion.2 = bf16[512,1024]{1,0:T(8,128)(2,1)} fusion(bf16[512,4096]{1,0:T(8,128)(2,1)} %all-gather.7.cloned.1.call-done, bf16[4096,1024]{1,0:T(8,128)(2,1)} %param.15), kind=kOutput, calls=%fused_computation.26 | convolution fusion | flops 4295491584 | bytes 13631488 | tf_op jit(solution)/shard_map/dot_general | solution.py:131
  56.8 1.9 reshape.173
  58.7 3.4 %convolution_bitcast_fusion.1 = f32[4,128,256]{2,1,0:T(8,128)} fusion(bf16[8,64,4,256]{3,2,1,0:T(4,128)(2,1)S(1)} %reshape.173, f32[4,8,64,128]{3,1,2,0:T(8,128)S(1)} %get-tuple-element.103, f32[8,64,4,128]{3,2,1,0:T(4,128)S(1)} %reshape.176, f32[4,8,128]{2,1,0:T(8,128)S(1)} %get-tuple-element.89, f32[4,128]{1,0:T(4,128)S(1)} %bitcast.264), kind=kOutput, calls=%fused_computation.33 | convolution fusion | flops 806092800 | bytes 3688448 | tf_op jit(solution)/shard_map/hncd,hncv->hdv/dot_general | solution.py:106
  62.1 0.0 all-gather.9.cloned.1.call-start
  62.2 9.4 %all-gather = f32[16,1,128]{2,1,0:T(1,128)S(1)} all-gather(f32[4,1,128]{2,1,0:T(1,128)S(1)} %get-tuple-element.80), channel_id=2, replica_groups=mesh['sp_0'=4,'sp_1'=4,'sp_2'=4,'tp'=2] {'sp_2'}, dimensions={0}, use_global_device_ids=true | all-gather | bytes 10240 | tf_op jit(solution)/shard_map/all_gather | solution.py:36
  71.6 10.1 %all_gather.31 = f32[4,4,128]{2,1,0:T(4,128)S(1)} all-gather(f32[1,4,128]{2,1,0:T(4,128)S(1)} %get-tuple-element.100), channel_id=1, replica_groups=mesh['sp_0'=4,'sp_1'=4,'sp_2'=4,'tp'=2] {'sp_1'}, dimensions={0}, use_global_device_ids=true | all-gather | bytes 10240 | tf_op jit(solution)/shard_map/all_gather | solution.py:36
  81.6 11.9 %all-gather.13.cloned.1.call-done = f32[16,128,256]{2,1,0:T(8,128)} async-done(((f32[4,128,256]{2,1,0:T(8,128)}), f32[16,128,256]{2,1,0:T(8,128)}) %all-gather.13.cloned.1.call-update) | async-done | bytes 2097168 | tf_op jit(solution)/shard_map/all_gather | solution.py:36
  93.5 2.7 %bitcast_add_fusion.5 = f32[1,4,128,256]{3,2,1,0:T(8,128)} fusion(f32[16,128,256]{2,1,0:T(8,128)} %all-gather.13.cloned.1.call-done, f32[4,128]{1,0:T(4,128)S(1)} %get-tuple-element.98, f32[4,128]{1,0:T(4,128)S(1)} %get-tuple-element.102, f32[4,128]{1,0:T(4,128)S(1)} %bitcast.262, f32[4,128]{1,0:T(4,128)S(1)} %get-tuple-element.101), kind=kLoop, calls=%fused_computation.70 | loop fusion | flops 917504 | bytes 2629632 | tf_op jit(solution)/shard_map/add | solution.py:65
  96.2 0.2 all-gather.11.cloned.1.call-start
  96.5 30.6 %all-gather.9.cloned.1.call-done = f32[4,4,128,256]{3,2,1,0:T(8,128)} async-done(((f32[1,4,128,256]{3,2,1,0:T(8,128)}), f32[4,4,128,256]{3,2,1,0:T(8,128)}) %all-gather.9.cloned.1.call-update) | async-done | bytes 2097168 | tf_op jit(solution)/shard_map/all_gather | solution.py:36
  127.1 2.6 %multiply_add_fusion = f32[1,4,128,256]{3,2,1,0:T(8,128)} fusion(f32[4,4,128,256]{3,2,1,0:T(8,128)} %all-gather.9.cloned.1.call-done, f32[4,128]{1,0:T(4,128)S(1)} %get-tuple-element.99, f32[4,128]{1,0:T(4,128)S(1)} %get-tuple-element.97, f32[4,128]{1,0:T(4,128)S(1)} %get-tuple-element.96, f32[4,128]{1,0:T(4,128)S(1)} %get-tuple-element.95), kind=kLoop, calls=%fused_computation.77 | loop fusion | flops 917504 | bytes 2629632 | tf_op jit(solution)/shard_map/add | solution.py:65
  129.8 0.0 reduce-scatter.2.cloned.1.call-start
  129.9 9.5 %all_gather.32 = f32[4,4,128]{2,1,0:T(4,128)S(1)} all-gather(f32[1,4,128]{2,1,0:T(4,128)S(1)} %get-tuple-element.94), channel_id=1, replica_groups=mesh['sp_0'=4,'sp_1'=4,'sp_2'=4,'tp'=2] {'sp_0'}, dimensions={0}, use_global_device_ids=true | all-gather | bytes 10240 | tf_op jit(solution)/shard_map/all_gather | solution.py:36
  139.4 1.6 convert_bitcast_fusion
  141.0 3.0 %convolution_select_fusion = f32[4,8,64,64]{3,2,1,0:T(8,128)} fusion(f32[4,8,64,128]{3,1,2,0:T(8,128)S(1)} %copy-done.5, f32[4,8,64,128]{3,1,2,0:T(8,128)S(1)} %copy-done.4, pred[64,64]{1,0:T(8,128)(4,1)S(1)} %iota_compare_fusion), kind=kOutput, calls=%fused_computation.27 | convolution fusion | flops 201457664 | bytes 2625536 | tf_op jit(solution)/shard_map/hnid,hnjd->hnij/dot_general | solution.py:76
  144.0 2.6 %bitcast_multiply_fusion = (f32[8,4,64,128]{3,0,2,1:T(8,128)}, f32[8,4,64,128]{3,0,2,1:T(8,128)}) fusion(f32[4,8,64,128]{3,1,2,0:T(8,128)S(1)} %get-tuple-element.103, f32[8,64,4,128]{3,2,1,0:T(4,128)S(1)} %copy-done.1, f32[8,4,128]{2,0,1:T(8,128)S(1)} %get-tuple-element.88, f32[8,64,4,128]{3,2,1,0:T(4,128)S(1)} %reshape.176), kind=kLoop, calls=%fused_computation.34 | loop fusion | flops 786432 | bytes 5259264 | tf_op jit(solution)/shard_map/mul | solution.py:71
  146.7 14.2 %all-gather.11.cloned.1.call-done = f32[4,4,128,256]{3,2,1,0:T(8,128)} async-done(((f32[1,4,128,256]{3,2,1,0:T(8,128)}), f32[4,4,128,256]{3,2,1,0:T(8,128)}) %all-gather.11.cloned.1.call-update) | async-done | bytes 2097168 | tf_op jit(solution)/shard_map/all_gather | solution.py:36
  160.8 3.4 %fusion.30 = f32[4,128,256]{2,1,0:T(8,128)S(1)} fusion(f32[4,4,128,256]{3,2,1,0:T(8,128)} %all-gather.11.cloned.1.call-done, f32[4,4,128,256]{3,2,1,0:T(8,128)} %all-gather.9.cloned.1.call-done, f32[16,128,256]{2,1,0:T(8,128)} %all-gather.13.cloned.1.call-done, f32[4,128]{1,0:T(4,128)S(1)} %get-tuple-element.98, f32[4,128]{1,0:T(4,128)S(1)} %get-tuple-element.102, ...), kind=kLoop, calls=%fused_computation.56 | loop fusion | flops 4849664 | bytes 6844428 | tf_op jit(solution)/shard_map/add | solution.py:65
  164.2 36.9 %while.12 = (s32[]{:T(128)}, f32[4,128,256]{2,1,0:T(8,128)S(1)}, f32[8,4,64,256]{3,2,0,1:T(8,128)}, f32[8,4,128]{2,0,1:T(8,128)S(1)}, f32[8,4,64,128]{3,0,2,1:T(...) while((s32[]{:T(128)}, f32[4,128,256]{2,1,0:T(8,128)S(1)}, ...), condition=%wide.region_4.5_spmd, body=%wide.region_3.4_spmd.sunk | while | flops 201588736 | bytes 2890845 | solution.py:95
  164.2 1.8 constant_dynamic-slice_fusion.5
  166.1 1.1 fusion.89
  167.2 1.7 convolution_add_fusion.2
  168.9 1.7 constant_dynamic-slice_fusion.5
  170.7 1.1 fusion.89
  171.8 1.7 convolution_add_fusion.2
  173.5 1.7 constant_dynamic-slice_fusion.5
  175.3 1.1 fusion.89
  176.4 1.7 convolution_add_fusion.2
  178.1 1.7 constant_dynamic-slice_fusion.5
  179.9 1.1 fusion.89
  181.0 1.7 convolution_add_fusion.2
  182.7 1.7 constant_dynamic-slice_fusion.5
  184.5 1.1 fusion.89
  185.6 1.7 convolution_add_fusion.2
  187.3 1.7 constant_dynamic-slice_fusion.5
  189.1 1.1 fusion.89
  190.2 1.7 convolution_add_fusion.2
  192.0 1.7 constant_dynamic-slice_fusion.5
  193.7 1.1 fusion.89
  194.8 1.7 convolution_add_fusion.2
  196.6 1.7 constant_dynamic-slice_fusion.5
  198.3 1.1 fusion.89
  199.5 1.7 convolution_add_fusion.2
  201.2 4.1 %multiply_reduce_fusion = (f32[8,64,4]{1,0,2:T(8,128)S(1)}, f32[8,64,4,256]{3,1,0,2:T(8,128)}) fusion(f32[8,4,64,256]{3,2,0,1:T(8,128)} %get-tuple-element.42, f32[4,8,64,64]{3,2,1,0:T(8,128)S(1)} %copy-done.6, bf16[8,64,4,256]{3,2,1,0:T(4,128)(2,1)S(1)} %reshape.173), kind=kOutput, calls=%fused_computation.23 | convolution fusion | flops 404224000 | bytes 5775360 | tf_op jit(solution)/shard_map/hnij,hnjv->hniv/dot_general | solution.py:78
  205.2 0.2 copy.62
  205.4 0.6 mul.402
  206.0 1.8 copy.73
  207.8 0.1 copy-done.2
  207.9 1.4 copy.58
  209.3 1.8 copy.72
  211.1 0.1 copy-done.7
  211.2 17.5 %convolution_convert_fusion = bf16[512,4096]{1,0:T(8,128)(2,1)} fusion(bf16[1024,4096]{1,0:T(8,128)(2,1)} %param.19, f32[512,1024]{1,0:T(8,128)} %bitcast.255, f32[512,1024]{1,0:T(8,128)S(1)} %bitcast.254, bf16[512,4096]{1,0:T(8,128)(2,1)} %all-gather.7.cloned.1.call-done, bf16[4096,1024]{1,0:T(8,128)(2,1)} %param.16, f32[1024]{0:T(1024)S(1)} %copy-done.9), kind=kOutput, calls=%fused_computation.9 | convolution fusion | flops 8597274624 | bytes 29364224 | tf_op jit(solution)/shard_map/dot_general | solution.py:173
  228.7 15.4 %reduce-scatter.2.cloned.1.call-done = bf16[256,4096]{1,0:T(8,128)(2,1)} async-done(((bf16[512,4096]{1,0:T(8,128)(2,1)}), bf16[256,4096]{1,0:T(8,128)(2,1)}) %reduce-scatter.2.cloned.1.call-update) | async-done | bytes 2097168 | tf_op jit(solution)/shard_map/reduce_scatter | solution.py:49
  (45 shorter events, 0.3 us)
Async XLA Ops:
  6.5 2.2 copy-start.3
  6.5 25.1 %all-gather.7.cloned.1.call-start = ((), (), s32[]{:S(2)}) async-start(), calls=%async_computation.1 | async-start | bytes 6291456 | tf_op jit(solution)/shard_map/all_gather | solution.py:22
  11.5 0.7 copy-start.8
  11.5 82.1 %all-gather.13.cloned.1.call-start = ((), (), s32[]{:S(2)}) async-start(), calls=%async_computation.5 | async-start | bytes 2621440 | tf_op jit(solution)/shard_map/all_gather | solution.py:36
  44.0 2.6 %copy-start = (f32[8,64,4,128]{3,2,1,0:T(4,128)}, f32[8,64,4,128]{3,2,1,0:T(4,128)S(1)}, u32[]{:S(2)}) copy-start(f32[8,64,4,128]{3,2,1,0:T(4,128)S(1)} %mul.334) | copy-start | bytes 3145732
  62.1 65.0 %all-gather.9.cloned.1.call-start = ((), (), s32[]{:S(2)}) async-start(), calls=%async_computation.2 | async-start | bytes 2621440 | tf_op jit(solution)/shard_map/all_gather | solution.py:36
  96.2 64.6 %all-gather.11.cloned.1.call-start = ((), (), s32[]{:S(2)}) async-start(), calls=%async_computation.3 | async-start | bytes 2621440 | tf_op jit(solution)/shard_map/all_gather | solution.py:36
  129.8 114.3 %reduce-scatter.2.cloned.1.call-start = ((), (), s32[]{:S(2)}) async-start(), calls=%async_computation.4 | async-start | bytes 6291456 | tf_op jit(solution)/shard_map/reduce_scatter | solution.py:49
  129.8 11.2 %copy-start.4 = (f32[4,8,64,128]{3,1,2,0:T(8,128)S(1)}, f32[4,8,64,128]{3,1,2,0:T(8,128)}, u32[]{:S(2)}) copy-start(f32[4,8,64,128]{3,1,2,0:T(8,128)} %get-tuple-element.84) | copy-start | bytes 3145732
  129.8 11.2 %copy-start.5 = (f32[4,8,64,128]{3,1,2,0:T(8,128)S(1)}, f32[4,8,64,128]{3,1,2,0:T(8,128)}, u32[]{:S(2)}) copy-start(f32[4,8,64,128]{3,1,2,0:T(8,128)} %get-tuple-element.85) | copy-start | bytes 3145732
  141.0 3.0 %copy-start.1 = (f32[8,64,4,128]{3,2,1,0:T(4,128)S(1)}, f32[8,64,4,128]{3,2,1,0:T(4,128)}, u32[]{:S(2)}) copy-start(f32[8,64,4,128]{3,2,1,0:T(4,128)} %copy-done) | copy-start | bytes 3145732
  164.2 37.0 %copy-start.6 = (f32[4,8,64,64]{3,2,1,0:T(8,128)S(1)}, f32[4,8,64,64]{3,2,1,0:T(8,128)}, u32[]{:S(2)}) copy-start(f32[4,8,64,64]{3,2,1,0:T(8,128)} %convolution_select_fusion) | copy-start | bytes 1572868
  206.0 1.9 copy-start.2
  209.3 1.9 copy-start.7
  209.3 1.9 copy-start.9
Sparse Core Ops, SparseCore 0:
  11.6 19.9 all-gather.6
  62.2 31.2 all-gather.12
  96.3 30.7 all-gather.8
  129.9 30.8 all-gather.10
  228.8 15.2 reduce-scatter.1
where the time goes:
time: 251 us
  waiting for transfers between devices  91.7 us (37%)
  matrix products  72.2 us (29%)
  blocking collectives  29 us (12%)
  local copies, waits for them, and re-layouts  23.2 us (9%)
  other arithmetic  20.6 us (8%)
  between operations  13.4 us (5%)
    all_gather x3, waiting for transfers between devices, carried_in_2(): pieces = jax.tree.map(lambda part: lax.all_gather(part, axis), total)  56.7 us
    all_gather x3, blocking collectives, carried_in_2(): pieces = jax.tree.map(lambda part: lax.all_gather(part, axis), total)  29 us
    dot_general x3, matrix products, project(): jnp.dot(row_piece, matrix, preferred_element_type=jnp.float32)  21.7 us
    all_gather x1, waiting for transfers between devices, gathered_then(): return work(lax.all_gather(shard, axis, axis=dim, tiled=True), jnp.int32(0))  19.5 us
    dot_general x1, matrix products, project_out(): jnp.dot(lax.dynamic_slice_in_dim(gated_rows, first_row, row_count, 0), ou...  17.5 us
    reduce_scatter x1, waiting for transfers between devices, own_rows(): lax.psum_scatter(sent, axis, scatter_dimension=0, tiled=True)  15.4 us
    dynamic_slice x16, local copies, waits for them, and re-layouts, local_pass(): final_state, carried_out = lax.scan(advance, start_state, sequence_inputs)  14.1 us
    dot_general x8, matrix products, advance(): jnp.einsum('hjd,hjv->hdv', key_now, value_now, precision=precise)  13.5 us
  transfers between devices with their start and end apart: 5, of which 5 were waited for; matrix products, arithmetic and copies ran while one was open for 3% of the time, Pallas kernels for 0%

commit v1 on v0

v1 whole, which is shorter than its diff:
```python
import functools
import math

import jax
import jax.numpy as jnp
from jax import lax
from jax.experimental import pallas as pl
from jax.experimental.pallas import tpu as pltpu
from jax.sharding import Mesh
from jax.sharding import PartitionSpec as P

HEAD_K = 128
HEAD_V = 256
AXES = ("z", "y1", "y0", "x", "tp")
SP = ("z", "y1", "y0", "x")
INNER = ("y1", "y0", "x")
OUTER = ("z",)
EPS = 1e-06
VMEM_LIMIT = 58 * 1024 * 1024
COLS = 256


def vmem(shape=None):
    return pl.BlockSpec(memory_space=pltpu.VMEM)


def hbm():
    return pl.BlockSpec(memory_space=pl.ANY)


def params(**more):
    return pltpu.CompilerParams(vmem_limit_bytes=VMEM_LIMIT, **more)


def kv_body(at_ref, x_hbm, gain_ref, ld_ref, wk_hbm, wv_hbm, *rest, second):
    if second:
        prev_ref = rest[0]
        rest = rest[4:]
    xn_hbm, k_hbm, v_hbm, s_ref, x_buf, xn_buf, wk_buf, wv_buf, k_buf, v_buf, sems, out_sems = rest
    rows, depth = x_buf.shape
    key_width, value_width = k_buf.shape[1], v_buf.shape[1]
    half = at_ref[1]
    copies = []
    in_x = pltpu.make_async_copy(x_hbm, x_buf, sems.at[0])
    in_x.start()
    for j in range(key_width // COLS):
        cut = pl.ds(j * COLS, COLS)
        copies.append(pltpu.make_async_copy(wk_hbm.at[:, cut], wk_buf.at[j], sems.at[1 + j]))
    key_steps = len(copies)
    for j in range(value_width // COLS):
        cut = pl.ds(j * COLS, COLS)
        copies.append(
            pltpu.make_async_copy(wv_hbm.at[:, cut], wv_buf.at[j], sems.at[1 + key_steps + j])
        )
    for copy in copies:
        copy.start()
    in_x.wait()
    step = 32

    def normalize(i, carry):
        cut = pl.ds(pl.multiple_of(i * step, step), step)
        x = x_buf[cut, :].astype(jnp.float32)
        scale = lax.rsqrt(jnp.mean(x * x, axis=-1, keepdims=True) + EPS)
        xn_buf[cut, :] = (x * scale * gain_ref[...]).astype(jnp.bfloat16)
        return carry

    lax.fori_loop(0, rows // step, normalize, 0)
    out_xn = pltpu.make_async_copy(xn_buf, xn_hbm.at[half], out_sems.at[0])
    out_xn.start()
    position = (at_ref[0] + 1 + lax.broadcasted_iota(jnp.int32, (rows, COLS), 0)).astype(jnp.float32)
    for j, copy in enumerate(copies):
        copy.wait()
        if j < key_steps:
            cut = slice(j * COLS, (j + 1) * COLS)
            acc = jnp.dot(xn_buf[...], wk_buf[j], preferred_element_type=jnp.float32)
            k_buf[:, cut] = (acc * jnp.exp(-ld_ref[:, cut] * position)).astype(jnp.bfloat16)
        else:
            i = j - key_steps
            acc = jnp.dot(xn_buf[...], wv_buf[i], preferred_element_type=jnp.float32)
            v_buf[:, i * COLS : (i + 1) * COLS] = acc.astype(jnp.bfloat16)
    out_k = pltpu.make_async_copy(k_buf, k_hbm.at[half], out_sems.at[1])
    out_v = pltpu.make_async_copy(v_buf, v_hbm.at[half], out_sems.at[2])
    out_k.start()
    out_v.start()
    for h in range(key_width // HEAD_K):
        state = lax.dot_general(
            k_buf[:, h * HEAD_K : (h + 1) * HEAD_K],
            v_buf[:, h * HEAD_V : (h + 1) * HEAD_V],
            (((0,), (0,)), ((), ())),
            preferred_element_type=jnp.float32,
        )
        if second:
            state = state + prev_ref[h]
        s_ref[h] = state.astype(s_ref.dtype)
    out_xn.wait()
    out_k.wait()
    out_v.wait()


def project_kv(at, x, gain, ld, wk, wv, before=None):
    rows, depth = x.shape
    kw, vw = wk.shape[1], wv.shape[1]
    heads = kw // HEAD_K
    second = before is not None
    bf = jnp.bfloat16
    shapes = (
        jax.ShapeDtypeStruct((2, rows, depth), bf),
        jax.ShapeDtypeStruct((2, rows, kw), bf),
        jax.ShapeDtypeStruct((2, rows, vw), bf),
        jax.ShapeDtypeStruct((heads, HEAD_K, HEAD_V), bf if second else jnp.float32),
    )
    in_specs = [pl.BlockSpec(memory_space=pltpu.SMEM), hbm(), vmem(), vmem(), hbm(), hbm()]
    args = [at, x, gain, ld, wk, wv]
    aliases = {}
    if second:
        in_specs += [vmem(), hbm(), hbm(), hbm()]
        args += [before[3], before[0], before[1], before[2]]
        aliases = {7: 0, 8: 1, 9: 2}
    return pl.pallas_call(
        functools.partial(kv_body, second=second),
        out_shape=shapes,
        in_specs=in_specs,
        out_specs=(hbm(), hbm(), hbm(), vmem()),
        scratch_shapes=[
            pltpu.VMEM((rows, depth), bf),
            pltpu.VMEM((rows, depth), bf),
            pltpu.VMEM((kw // COLS, depth, COLS), bf),
            pltpu.VMEM((vw // COLS, depth, COLS), bf),
            pltpu.VMEM((rows, kw), bf),
            pltpu.VMEM((rows, vw), bf),
            pltpu.SemaphoreType.DMA((1 + (kw + vw) // COLS,)),
            pltpu.SemaphoreType.DMA((3,)),
        ],
        input_output_aliases=aliases,
        compiler_params=params(),
        name="kv_second" if second else "kv_first",
    )(*args)


def q_body(at_ref, xn_ref, w_ref, ld_ref, q_ref):
    rows = xn_ref.shape[0]
    position = (at_ref[0] + 1 + lax.broadcasted_iota(jnp.int32, (rows, COLS), 0)).astype(jnp.float32)
    acc = jnp.dot(xn_ref[...], w_ref[...], preferred_element_type=jnp.float32)
    q_ref[...] = (acc * (jnp.exp(ld_ref[...] * position) * HEAD_K ** (-0.5))).astype(jnp.bfloat16)


def g_body(xn_ref, w_ref, gain_ref, g_ref):
    acc = jnp.dot(xn_ref[...], w_ref[...], preferred_element_type=jnp.float32)
    g_ref[...] = (acc * gain_ref[...] / (1.0 + jnp.exp(-acc))).astype(jnp.bfloat16)


def project_q(at, xn, w, ld):
    rows, depth = xn.shape
    width = w.shape[1]
    return pl.pallas_call(
        q_body,
        out_shape=jax.ShapeDtypeStruct((rows, width), jnp.bfloat16),
        grid_spec=pltpu.PrefetchScalarGridSpec(
            num_scalar_prefetch=1,
            grid=(width // COLS,),
            in_specs=[
                pl.BlockSpec((rows, depth), lambda j, at: (0, 0), pipeline_mode=pl.Buffered(1)),
                pl.BlockSpec((depth, COLS), lambda j, at: (0, j)),
                pl.BlockSpec((1, COLS), lambda j, at: (0, j)),
            ],
            out_specs=pl.BlockSpec((rows, COLS), lambda j, at: (0, j)),
        ),
        compiler_params=params(),
        name="project_q",
    )(at, xn, w, ld)


def project_g(xn, w, gain):
    rows, depth = xn.shape
    width = w.shape[1]
    return pl.pallas_call(
        g_body,
        out_shape=jax.ShapeDtypeStruct((rows, width), jnp.bfloat16),
        grid=(width // COLS,),
        in_specs=[
            pl.BlockSpec((rows, depth), lambda j: (0, 0), pipeline_mode=pl.Buffered(1)),
            pl.BlockSpec((depth, COLS), lambda j: (0, j)),
            pl.BlockSpec((1, COLS), lambda j: (0, j)),
        ],
        out_specs=pl.BlockSpec((rows, COLS), lambda j: (0, j)),
        compiler_params=params(),
        name="project_g",
    )(xn, w, gain)


def local_body(q_ref, k_ref, v_ref, o_ref):
    rows = q_ref.shape[0]
    half = rows // 2
    f32 = jnp.float32
    nt = (((1,), (1,)), ((), ()))
    row = lax.broadcasted_iota(jnp.int32, (half, half), 0)
    col = lax.broadcasted_iota(jnp.int32, (half, half), 1)
    keep = row >= col
    for i in range(2):
        q = q_ref[i * half : (i + 1) * half, :]
        total = None
        for j in range(i + 1):
            part = slice(j * half, (j + 1) * half)
            scores = lax.dot_general(q, k_ref[part, :], nt, preferred_element_type=f32)
            if i == j:
                scores = jnp.where(keep, scores, 0.0)
            piece = jnp.dot(scores.astype(jnp.bfloat16), v_ref[part, :], preferred_element_type=f32)
            total = piece if total is None else total + piece
        o_ref[i * half : (i + 1) * half, :] = total


def attend_local(q, k, v):
    rows = q.shape[0]
    heads = q.shape[1] // HEAD_K
    return pl.pallas_call(
        local_body,
        out_shape=jax.ShapeDtypeStruct((rows, heads * HEAD_V), jnp.float32),
        grid=(heads,),
        in_specs=[
            pl.BlockSpec((rows, HEAD_K), lambda h: (0, h)),
            pl.BlockSpec((rows, HEAD_K), lambda h: (0, h)),
            pl.BlockSpec((rows, HEAD_V), lambda h: (0, h)),
        ],
        out_specs=pl.BlockSpec((rows, HEAD_V), lambda h: (0, h)),
        compiler_params=params(),
        name="attend_local",
    )(q, k, v)


def gate_rows(q, carried, local, gate):
    attended = local + jnp.dot(q, carried, preferred_element_type=jnp.float32)
    scale = lax.rsqrt(jnp.mean(attended * attended, axis=-1, keepdims=True) + EPS)
    return (attended * scale * gate.astype(jnp.float32)).astype(jnp.bfloat16)


def gate_body(at_ref, q_ref, s_ref, o_ref, g_ref, out_ref):
    out_ref[...] = gate_rows(q_ref[0], s_ref[0], o_ref[0], g_ref[0])


def gate_half(at, q, carried, local, gate):
    rows = q.shape[0] // 2
    heads = q.shape[1] // HEAD_K
    return pl.pallas_call(
        gate_body,
        out_shape=jax.ShapeDtypeStruct((rows, heads * HEAD_V), jnp.bfloat16),
        grid_spec=pltpu.PrefetchScalarGridSpec(
            num_scalar_prefetch=1,
            grid=(heads,),
            in_specs=[
                pl.BlockSpec((1, rows, HEAD_K), lambda h, at: (at[1], 0, h)),
                pl.BlockSpec((1, HEAD_K, HEAD_V), lambda h, at: (h, 0, 0)),
                pl.BlockSpec((1, rows, HEAD_V), lambda h, at: (at[1], 0, h)),
                pl.BlockSpec((1, rows, HEAD_V), lambda h, at: (at[1], 0, h)),
            ],
            out_specs=pl.BlockSpec((rows, HEAD_V), lambda h, at: (0, h)),
        ),
        compiler_params=params(),
        name="gate_half",
    )(at, q.reshape(2, rows, -1), carried, local.reshape(2, rows, -1), gate.reshape(2, rows, -1))


def out_own_body(a_ref, w_ref, o_ref):
    o_ref[...] = jnp.dot(a_ref[...], w_ref[...], preferred_element_type=jnp.float32)


def out_own(a, w):
    rows, depth = a.shape
    width = w.shape[1]
    cols = 512
    return pl.pallas_call(
        out_own_body,
        out_shape=jax.ShapeDtypeStruct((rows, width), jnp.float32),
        grid=(width // cols,),
        in_specs=[
            pl.BlockSpec((rows, depth), lambda j: (0, 0), pipeline_mode=pl.Buffered(1)),
            pl.BlockSpec((depth, cols), lambda j: (0, j)),
        ],
        out_specs=pl.BlockSpec((rows, cols), lambda j: (0, j)),
        compiler_params=params(),
        name="out_own",
    )(a, w)


def out_add_body(a_ref, w_ref, p_ref, o_ref):
    o_ref[...] = (
        p_ref[...] + jnp.dot(a_ref[...], w_ref[...], preferred_element_type=jnp.float32)
    ).astype(jnp.bfloat16)


def out_add(a, w, partial):
    rows, depth = a.shape
    width = w.shape[1]
    cols = 512
    return pl.pallas_call(
        out_add_body,
        out_shape=jax.ShapeDtypeStruct((rows, width), jnp.bfloat16),
        grid=(width // cols,),
        in_specs=[
            pl.BlockSpec((rows, depth), lambda j: (0, 0), pipeline_mode=pl.Buffered(1)),
            pl.BlockSpec((depth, cols), lambda j: (0, j)),
            pl.BlockSpec((rows, cols), lambda j: (0, j)),
        ],
        out_specs=pl.BlockSpec((rows, cols), lambda j: (0, j)),
        compiler_params=params(),
        name="out_add",
    )(a, w, partial)


def swap(x):
    return lax.ppermute(x, "tp", [(0, 1), (1, 0)])


def tied(*xs):
    return lax.optimization_barrier(xs)


def on_device(tokens, norm_gain, wq, wk, wv, wg, decay_bias, head_gain, wo):
    rows = tokens.shape[0]
    kw = wk.shape[1]
    heads = kw // HEAD_K
    tp = lax.axis_index("tp")
    stretch = lax.axis_index(SP)
    start = (stretch * (2 * rows)).astype(jnp.int32)
    sequence = lax.axis_size(SP) * 2 * rows
    logits = decay_bias.astype(jnp.float32) + math.log(sequence / 8.0)
    ld = (jax.nn.log_sigmoid(logits) / 16.0).reshape(1, kw)
    gain = norm_gain.astype(jnp.float32).reshape(1, -1)
    other_tokens = swap(tokens)

    def place(half):
        return jnp.stack([start + half * rows, half]).astype(jnp.int32)

    at_own, at_other = place(tp), place(1 - tp)
    first = project_kv(at_own, tokens, gain, ld, wk, wv)
    other_tokens, wo_send = tied(other_tokens, wo)
    other_wo = swap(wo_send)
    xn, k, v, state = project_kv(at_other, other_tokens, gain, ld, wk, wv, first)
    xn, k, v = (t.reshape(2 * rows, -1) for t in (xn, k, v))

    inner = lax.axis_size(INNER)
    pieces = state.reshape(inner, heads * HEAD_K // inner, HEAD_V)
    got = lax.all_to_all(pieces, INNER, 0, 0, tiled=True)
    q = project_q(place(0 * tp), xn, wq, ld)
    local = attend_local(q, k, v)
    got, local = tied(got, local)
    got = got.astype(jnp.float32)
    total = got.sum(0).astype(jnp.bfloat16)
    outer = lax.axis_size(OUTER)
    totals = lax.all_to_all(
        jnp.broadcast_to(total[None], (outer,) + total.shape), OUTER, 0, 0, tiled=True
    )
    xn, local = tied(xn, local)
    gate = project_g(xn, wg, head_gain.astype(jnp.float32).reshape(1, -1))
    totals, gate = tied(totals, gate)
    passed = (jnp.arange(outer) < lax.axis_index(OUTER))[:, None, None]
    far = jnp.where(passed, totals.astype(jnp.float32), 0.0).sum(0)
    run = far
    before = []
    for j in range(inner):
        before.append(run.astype(jnp.bfloat16))
        run = run + got[j]
    carried = lax.all_to_all(jnp.stack(before), INNER, 0, 0, tiled=True)
    carried = carried.reshape(heads, HEAD_K, HEAD_V)

    theirs = gate_half(at_other, q, carried, local, gate)
    received = swap(theirs)
    mine = gate_half(at_own, q, carried, local, gate)
    partial = out_own(mine, wo)
    return out_add(received, other_wo, partial)


def solution(mesh):
    z, y, x = 4, 4, 4
    finer = Mesh(mesh.devices.reshape(z, 2, 2, x, mesh.shape["tp"]), AXES)
    rows = P(AXES, None)
    cols = P(None, "tp")
    in_specs = (rows, P(), cols, cols, cols, cols, P("tp"), P("tp"), P("tp", None))
    return jax.shard_map(
        on_device, mesh=finer, in_specs=in_specs, out_specs=rows, check_vma=False
    )
```

time: 251 us -> 116 us (0.46)
  waiting for transfers between devices: 91.7 us -> 4.01 us
  Pallas kernels: 0 us -> 75.4 us
  matrix products: 72.2 us -> 0 us
  local copies, waits for them, and re-layouts: 23.2 us -> 1.45 us
  other arithmetic: 20.6 us -> 3.67 us
  starting transfers between devices: 0.35 us -> 16 us
  blocking collectives: 29 us -> 14.1 us
  between operations: 13.4 us -> 0.17 us
    all_gather x4 -> x0, waiting for transfers between devices: 76.2 us -> none  [the longest x3 56.7 us: carried_in_2(): pieces = jax.tree.map(lambda part: lax.all_gather(part, axis), total)]
    pallas_call x0 -> x9, Pallas kernels: none -> 75.4 us  [the longest x2 25.8 us: project_kv(): pl.pallas_call(functools.partial(kv_body, second=second), out_shape=shape...]
    dot_general x23 -> x0, matrix products: 72.2 us -> none  [the longest x3 21.7 us: project(): jnp.dot(row_piece, matrix, preferred_element_type=jnp.float32)]
    all_gather x3 -> x0, blocking collectives: 29 us -> none  [carried_in_2(): pieces = jax.tree.map(lambda part: lax.all_gather(part, axis), total)]
    reduce_scatter x1 -> x0, waiting for transfers between devices: 15.4 us -> none  [own_rows(): lax.psum_scatter(sent, axis, scatter_dimension=0, tiled=True)]
    all_to_all x0 -> x1, blocking collectives: none -> 14.1 us  [on_device(): carried = lax.all_to_all(jnp.stack(before), INNER, 0, 0, tiled=True)]
    dynamic_slice x16 -> x0, local copies, waits for them, and re-layouts: 14.1 us -> none  [local_pass(): final_state, carried_out = lax.scan(advance, start_state, sequence_inputs)]
    all_to_all x0 -> x2, starting transfers between devices: none -> 11.9 us  [the longest x1 6.91 us: on_device(): got = lax.all_to_all(pieces, INNER, 0, 0, tiled=True)]
  transfers between devices with their start and end apart: 5 -> 5, of which waited for: 5 -> 1; matrix products, arithmetic and copies ran while one was open for 3% -> 4% of each run, Pallas kernels for 0% -> 58%
where the time goes in v1:
time: 116 us; the launch traced here: 115 us
  Pallas kernels  75.4 us (65%)
  starting transfers between devices  16 us (14%)
  blocking collectives  14.1 us (12%)
  waiting for transfers between devices  4.01 us (3%)
  other arithmetic  3.67 us (3%)
  local copies, waits for them, and re-layouts  1.45 us (1%)
    pallas_call x2, Pallas kernels, project_kv(): pl.pallas_call(functools.partial(kv_body, second=second), out_shape=shape...  25.8 us
    all_to_all x1, blocking collectives, on_device(): carried = lax.all_to_all(jnp.stack(before), INNER, 0, 0, tiled=True)  14.1 us
    pallas_call x2, Pallas kernels, gate_half(): pl.pallas_call(gate_body, out_shape=jax.ShapeDtypeStruct((rows, heads * H...  9.42 us
    pallas_call x1, Pallas kernels, out_add(): pl.pallas_call(out_add_body, out_shape=jax.ShapeDtypeStruct((rows, width)...  9.35 us
    pallas_call x1, Pallas kernels, project_g(): pl.pallas_call(g_body, out_shape=jax.ShapeDtypeStruct((rows, width), jnp....  9.26 us
    pallas_call x1, Pallas kernels, out_own(): pl.pallas_call(out_own_body, out_shape=jax.ShapeDtypeStruct((rows, width)...  9.19 us
    pallas_call x1, Pallas kernels, project_q(): pl.pallas_call(q_body, out_shape=jax.ShapeDtypeStruct((rows, width), jnp....  7.38 us
    all_to_all x1, starting transfers between devices, on_device(): got = lax.all_to_all(pieces, INNER, 0, 0, tiled=True)  6.91 us
  transfers between devices with their start and end apart: 5, of which 1 were waited for; matrix products, arithmetic and copies ran while one was open for 4% of the time, Pallas kernels for 58%

profile of v1, /device:TPU:1, one launch (start us, length us, event | category | flops | bytes accessed | tf_op | source)
XLA Modules:
  0.0 114.8 jit_solution(15461790093345099355)
XLA Ops:
  0.0 1.4 %collective-permute-start = (bf16[256,4096]{1,0:T(8,128)(2,1)}, bf16[256,4096]{1,0:T(8,128)(2,1)S(1)}, u32[]{:S(2)}, u32[]{:S(2)}) collective-permute-start(bf16[256,4096]{1,0:T(8,128)(2,1)} %x_hbm.1), channel_id=1, source_target_pairs={{0,1},{1,0},{2,3},{3,2},{4,5},{5,4},{6,7},{7,6},{8,9},{9,8},{10,11... | collective-permute-start | bytes 6291464 | tf_op jit(solution)/shard_map/ppermute | solution.py:310
  1.4 4.0 %collective-permute-done.x_hbm = bf16[256,4096]{1,0:T(8,128)(2,1)S(1)} collective-permute-done((bf16[256,4096]{1,0:T(8,128)(2,1)}, bf16[256,4096]{1,0:T(8,128)(2,1)S(1)}, u32[]{:S(2)}, u32[]{:S(2)}) %collective-permute-start) | collective-permute-done | bytes 2097184 | tf_op jit(solution)/shard_map/ppermute | solution.py:310
  5.4 0.0 copy-start
  5.4 0.4 collective-permute-start.2
  5.7 0.9 pad_add_fusion.2.at_ref
  6.6 1.3 %fusion.2 = f32[512]{0:T(512)} fusion(f32[512]{0:T(512)} %param.15), kind=kLoop, calls=%fused_computation.36 | loop fusion | flops 5120 | bytes 4096 | tf_op jit(solution)/shard_map/div | solution.py:326
  7.9 12.8 %kv_first.1 = (bf16[2,256,4096]{2,1,0:T(8,128)(2,1)}, bf16[2,256,512]{2,1,0:T(8,128)(2,1)}, bf16[2,256,1024]{2,1,0:T(8,128)(2,1)}, f32[4,128,256]{2,1,0:T(8,128)}) custom-call(s32[2]{0:T(128)} %pad_add_fusion.2.at_ref, bf16[256,4096]{1,0:T(8,128)(2,1)} %x_hbm.1, f32[1,4096]{1,0:T(1,128)} %bitcast.39, f32[1,512]{1,0:T(1,128)} %bitcast.41, ...), custom_call_target="tpu_custom_call" | custom-call | tf_op jit(solution)/shard_map/kv_first/pallas_call | solution.py:119
  20.7 0.0 copy-done
  20.7 0.6 pad_add_fusion.at_ref
  21.3 13.1 %kv_second.1 = (bf16[2,256,4096]{2,1,0:T(8,128)(2,1)}, bf16[2,256,512]{2,1,0:T(8,128)(2,1)}, bf16[2,256,1024]{2,1,0:T(8,128)(2,1)}, bf16[4,128,256]{2,1,0:T(8,128)(2,1)}) custom-call(s32[2]{0:T(128)} %pad_add_fusion.at_ref, bf16[256,4096]{1,0:T(8,128)(2,1)} %copy-done, ...), custom_call_target="tpu_custom_call", output_to_operand_aliasing={{0}: (7, {}), {1}: (8, {}), {2}: (9, {})} | custom-call | tf_op jit(solution)/shard_map/kv_second/pallas_call | solution.py:119
  34.4 6.9 %all-to-all-start = ((bf16[16,32,256]{2,1,0:T(8,128)(2,1)}), bf16[16,32,256]{2,1,0:T(8,128)(2,1)S(1)}, u32[]{:S(2)}, u32[]{:S(2)}) async-start(bf16[16,32,256]{2,1,0:T(8,128)(2,1)} %bitcast.38), calls=%async_computation | async-start | bytes 524288 | tf_op jit(solution)/shard_map/all_to_all | solution.py:342
  41.3 0.6 pad_add_fusion.1.at_ref
  41.9 7.4 %project_q.1.q_ref = bf16[512,512]{1,0:T(8,128)(2,1)} custom-call(s32[2]{0:T(128)} %pad_add_fusion.1.at_ref, bf16[512,4096]{1,0:T(8,128)(2,1)} %bitcast.26, bf16[4096,512]{1,0:T(8,128)(2,1)} %w_ref.3, f32[1,512]{1,0:T(1,128)} %bitcast.43), custom_call_target="tpu_custom_call" | custom-call | tf_op jit(solution)/shard_map/project_q/pallas_call | solution.py:155
  49.3 5.0 %attend_local.1 = f32[512,1024]{1,0:T(8,128)} custom-call(bf16[512,512]{1,0:T(8,128)(2,1)} %project_q.1.q_ref, bf16[512,512]{1,0:T(8,128)(2,1)} %bitcast.37, bf16[512,1024]{1,0:T(8,128)(2,1)} %bitcast.34), custom_call_target="tpu_custom_call" | custom-call | tf_op jit(solution)/shard_map/attend_local/pallas_call | solution.py:215
  54.3 0.0 all-to-all-done
  54.3 0.1 fusion.3
  54.3 0.6 broadcast_in_dim.20
  55.0 5.0 %all-to-all-start.1 = ((bf16[4,32,256]{2,1,0:T(8,128)(2,1)}), bf16[4,32,256]{2,1,0:T(8,128)(2,1)S(1)}, u32[]{:S(2)}, u32[]{:S(2)}) async-start(bf16[4,32,256]{2,1,0:T(8,128)(2,1)} %broadcast_in_dim.20), calls=%async_computation.1 | async-start | bytes 131072 | tf_op jit(solution)/shard_map/all_to_all | solution.py:349
  60.0 9.3 %project_g.1 = bf16[512,1024]{1,0:T(8,128)(2,1)} custom-call(bf16[512,4096]{1,0:T(8,128)(2,1)} %bitcast.27, bf16[4096,1024]{1,0:T(8,128)(2,1)} %w_ref.4, f32[1,1024]{1,0:T(1,128)} %bitcast.44), custom_call_target="tpu_custom_call" | custom-call | tf_op jit(solution)/shard_map/project_g/pallas_call | solution.py:176
  69.3 0.0 all-to-all-done.1
  69.3 0.1 select_reduce_fusion
  69.6 14.1 %all_to_all.15 = bf16[16,32,256]{2,1,0:T(8,128)(2,1)} all-to-all(bf16[16,32,256]{2,1,0:T(8,128)(2,1)S(1)} %constant_dynamic-update-slice_fusion), channel_id=1, replica_groups=mesh['z'=4,'y1'=2,'y0'=2,'x'=4,'tp'=2] {'y1','y0','x'}, dimensions={0} | all-to-all | bytes 524288 | tf_op jit(solution)/shard_map/all_to_all | solution.py:362
  83.7 4.7 %gate_half.2 = bf16[256,1024]{1,0:T(8,128)(2,1)} custom-call(s32[2]{0:T(128)} %pad_add_fusion.at_ref, bf16[2,256,512]{2,1,0:T(8,128)(2,1)} %bitcast.32, bf16[4,128,256]{2,1,0:T(8,128)(2,1)} %bitcast.35, f32[2,256,1024]{2,1,0:T(8,128)} %bitcast.28, bf16[2,256,1024]{2,1,0:T(8,128)(2,1)} %bitcast.30), custom_call_target="tpu_custom_call" | custom-call | tf_op jit(solution)/shard_map/gate_half/pallas_call | solution.py:243
  88.4 2.3 %collective-permute-start.1 = (bf16[256,1024]{1,0:T(8,128)(2,1)}, bf16[256,1024]{1,0:T(8,128)(2,1)S(1)}, u32[]{:S(2)}, u32[]{:S(2)}) collective-permute-start(bf16[256,1024]{1,0:T(8,128)(2,1)} %gate_half.2), channel_id=1, source_target_pairs={{0,1},{1,0},{2,3},{3,2},{4,5},{5,4},{6,7},{7,6},{8,9},{9,8},{10,11... | collective-permute-start | bytes 1572872 | tf_op jit(solution)/shard_map/ppermute | solution.py:310
  90.7 4.7 %gate_half.3.a_ref = bf16[256,1024]{1,0:T(8,128)(2,1)} custom-call(s32[2]{0:T(128)} %pad_add_fusion.2.at_ref, bf16[2,256,512]{2,1,0:T(8,128)(2,1)} %bitcast.33, bf16[4,128,256]{2,1,0:T(8,128)(2,1)} %bitcast.36, f32[2,256,1024]{2,1,0:T(8,128)} %bitcast.29, bf16[2,256,1024]{2,1,0:T(8,128)(2,1)} %bitcast.31), custom_call_target="tpu_custom_call" | custom-call | tf_op jit(solution)/shard_map/gate_half/pallas_call | solution.py:243
  95.4 9.2 %out_own.1.p_ref = f32[256,4096]{1,0:T(8,128)} custom-call(bf16[256,1024]{1,0:T(8,128)(2,1)} %gate_half.3.a_ref, bf16[1024,4096]{1,0:T(8,128)(2,1)} %w_ref.5), custom_call_target="tpu_custom_call" | custom-call | tf_op jit(solution)/shard_map/out_own/pallas_call | solution.py:270
  104.6 0.0 collective-permute-done.1.a_ref
  104.6 0.0 copy-start.1
  104.6 0.0 collective-permute-done.2.w_ref
  104.6 0.8 copy-done.1
  105.5 9.3 %out_add.1 = bf16[256,4096]{1,0:T(8,128)(2,1)} custom-call(bf16[256,1024]{1,0:T(8,128)(2,1)} %copy-done.1, bf16[1024,4096]{1,0:T(8,128)(2,1)} %collective-permute-done.2.w_ref, f32[256,4096]{1,0:T(8,128)} %out_own.1.p_ref), custom_call_target="tpu_custom_call" | custom-call | tf_op jit(solution)/shard_map/out_add/pallas_call | solution.py:294
  (17 shorter events, 0.2 us)
Async XLA Ops:
  0.0 5.4 %collective-permute-start = (bf16[256,4096]{1,0:T(8,128)(2,1)}, bf16[256,4096]{1,0:T(8,128)(2,1)S(1)}, u32[]{:S(2)}, u32[]{:S(2)}) collective-permute-start(bf16[256,4096]{1,0:T(8,128)(2,1)} %x_hbm.1), channel_id=1, source_target_pairs={{0,1},{1,0},{2,3},{3,2},{4,5},{5,4},{6,7},{7,6},{8,9},{9,8},{10,11... | collective-permute-start | bytes 6291464 | tf_op jit(solution)/shard_map/ppermute | solution.py:310
  5.4 15.4 %copy-start = (bf16[256,4096]{1,0:T(8,128)(2,1)}, bf16[256,4096]{1,0:T(8,128)(2,1)S(1)}, u32[]{:S(2)}) copy-start(bf16[256,4096]{1,0:T(8,128)(2,1)S(1)} %collective-permute-done.x_hbm) | copy-start | bytes 6291460
  5.4 99.3 %collective-permute-start.2 = (bf16[1024,4096]{1,0:T(8,128)(2,1)}, bf16[1024,4096]{1,0:T(8,128)(2,1)}, u32[]{:S(2)}, u32[]{:S(2)}) collective-permute-start(bf16[1024,4096]{1,0:T(8,128)(2,1)} %w_ref.5), channel_id=1, source_target_pairs={{0,1},{1,0},{2,3},{3,2},{4,5},{5,4},{6,7},{7,6},{8,9},{9,8},{10,11... | collective-permute-start | bytes 25165832 | tf_op jit(solution)/shard_map/ppermute | solution.py:310
  34.4 19.9 %all-to-all-start = ((bf16[16,32,256]{2,1,0:T(8,128)(2,1)}), bf16[16,32,256]{2,1,0:T(8,128)(2,1)S(1)}, u32[]{:S(2)}, u32[]{:S(2)}) async-start(bf16[16,32,256]{2,1,0:T(8,128)(2,1)} %bitcast.38), calls=%async_computation | async-start | bytes 524288 | tf_op jit(solution)/shard_map/all_to_all | solution.py:342
  55.0 14.3 %all-to-all-start.1 = ((bf16[4,32,256]{2,1,0:T(8,128)(2,1)}), bf16[4,32,256]{2,1,0:T(8,128)(2,1)S(1)}, u32[]{:S(2)}, u32[]{:S(2)}) async-start(bf16[4,32,256]{2,1,0:T(8,128)(2,1)} %broadcast_in_dim.20), calls=%async_computation.1 | async-start | bytes 131072 | tf_op jit(solution)/shard_map/all_to_all | solution.py:349
  88.4 16.2 %collective-permute-start.1 = (bf16[256,1024]{1,0:T(8,128)(2,1)}, bf16[256,1024]{1,0:T(8,128)(2,1)S(1)}, u32[]{:S(2)}, u32[]{:S(2)}) collective-permute-start(bf16[256,1024]{1,0:T(8,128)(2,1)} %gate_half.2), channel_id=1, source_target_pairs={{0,1},{1,0},{2,3},{3,2},{4,5},{5,4},{6,7},{7,6},{8,9},{9,8},{10,11... | collective-permute-start | bytes 1572872 | tf_op jit(solution)/shard_map/ppermute | solution.py:310
  104.6 0.8 copy-start.1
